TPU v7x, 32 devices: a whole 2x2x4 slice. The times are simulated.
32 devices in a mesh: sp: 8 (over z, x), tp: 4 (over y, core).
Axes of the slice: x: 2, y: 2, z: 4, core: 2. Of those that a mesh axis runs over, the one named last changes fastest.
Arguments:
- tokens: bfloat16 [4096, 2048], P(('sp', 'tp')), may hold values from -6 to 6
- norm_gain: float32 [2048], replicated, may hold values from 0.1 to 1.9
- w_query: bfloat16 [2048, 1024], P(None, 'tp'), may hold values from -16 to 16
- w_key: bfloat16 [2048, 1024], P(None, 'tp'), may hold values from -16 to 16
- w_value: bfloat16 [2048, 1024], P(None, 'tp'), may hold values from -0.125 to 0.125
- conv_in: bfloat16 [2048, 2048], P(None, 'tp'), may hold values from -0.125 to 0.125
- conv_gate: bfloat16 [2048, 2048], P(None, 'tp'), may hold values from -0.125 to 0.125
- conv_taps: float32 [31, 2048], P(None, 'tp'), may hold values from -3.7 to 3.7
- conv_gain: float32 [2048], P('tp'), may hold values from 0.1 to 1.9
- cum_gate: float32 [16, 4096], P('tp'), may hold values from -514 to 0, as said below
- out_attn: bfloat16 [1024, 2048], P('tp'), may hold values from -0.75 to 0.75
- out_conv: bfloat16 [2048, 2048], P('tp'), may hold values from -0.125 to 0.125
Outputs:
- mixed: bfloat16 [4096, 2048], P(('sp', 'tp'))
- log_total: float32 [16, 4096], P('tp', 'sp')
Inputs may be any that keep to these rules, and one draw needn't show every extreme that they name: `cum_gate`: for each head the values never rise from one position to the next and are at most 0.
All inputs are finite; a program needn't handle non-finite values.
Results may differ from a plain program's by a relative error of at most 0.014.
Values may be sent and summed in bfloat16 or wider, within the bound.
A program may use at most 128 MiB of HBM per device.

v0:
```python
import jax
import jax.numpy as jnp
from jax import lax
from jax.sharding import PartitionSpec as P

HEAD = 64


def shifted(array, axis, by):
    length = lax.axis_size(axis)
    pairs = [(i, i + by) for i in range(length) if 0 <= i + by < length]
    return lax.ppermute(array, axis, pairs)


def per_device(
    tokens,
    norm_gain,
    w_query,
    w_key,
    w_value,
    conv_in,
    conv_gate,
    conv_taps,
    conv_gain,
    cum_gate,
    out_attn,
    out_conv,
):
    heads_here = w_query.shape[1] // HEAD
    width_att = w_query.shape[1]
    channels = conv_in.shape[1]
    kernel_len = conv_taps.shape[0]
    wide = lax.all_gather(tokens, "tp", axis=0, tiled=True).astype(jnp.float32)
    factor = lax.rsqrt(jnp.mean(wide * wide, axis=1, keepdims=True) + 1e-06)
    normed = (wide * factor * norm_gain[None, :]).astype(jnp.bfloat16)
    query = (jnp.dot(normed, w_query, preferred_element_type=jnp.float32) * HEAD ** (-0.5)).astype(
        jnp.bfloat16
    )
    keyed = jnp.dot(normed, w_key, preferred_element_type=jnp.float32).astype(jnp.bfloat16)
    valued = jnp.dot(normed, w_value, preferred_element_type=jnp.float32).astype(jnp.bfloat16)
    opened = jnp.dot(normed, conv_in, preferred_element_type=jnp.float32)
    gating = jnp.dot(normed, conv_gate, preferred_element_type=jnp.float32)
    gated_rows = (opened * jax.nn.sigmoid(gating)).astype(jnp.bfloat16)
    joined = jnp.concatenate([query, keyed, valued, gated_rows], axis=1)
    local_rows = joined.shape[0]
    own_index = lax.axis_index("sp")
    offset = own_index * local_rows
    query_rows = joined[:, :width_att]
    key_rows = joined[:, width_att : 2 * width_att]
    value_rows = joined[:, 2 * width_att : 3 * width_att]
    gated = joined[:, 3 * width_att :]
    group_list = (query_rows, offset)
    group_data = []
    group_rows, group_start = group_list
    count_rows = group_rows.shape[0]
    group_data.append(
        (
            group_rows.reshape(count_rows, heads_here, HEAD),
            lax.dynamic_slice_in_dim(cum_gate, group_start, count_rows, 1),
            group_start + jnp.arange(count_rows, dtype=jnp.int32),
            group_start + count_rows - 1,
        )
    )

    def absorb(carry_in, group, key_block, value_block, first_place):
        query_heads, cum_query, query_place, last_query = group
        row_best, row_total, row_accum = carry_in
        length_in = key_block.shape[0]
        key_heads = key_block.reshape(length_in, heads_here, HEAD)
        value_heads = value_block.reshape(length_in, heads_here, HEAD)
        cum_keys = lax.dynamic_slice_in_dim(cum_gate, first_place, length_in, 1)
        scores = jnp.einsum(
            "qhd,khd->hqk", query_heads, key_heads, preferred_element_type=jnp.float32
        )
        scores = scores + cum_query[:, :, None] - cum_keys[:, None, :]
        key_place = first_place + jnp.arange(length_in, dtype=jnp.int32)
        visible = jnp.logical_and(
            key_place[None, :] <= query_place[:, None], key_place[None, :] >= 0
        )[None]
        scores = jnp.where(visible, scores, -1e30)
        new_best = jnp.maximum(row_best, jnp.max(scores, axis=2))
        shrink = jnp.exp(row_best - new_best)
        weights = jnp.where(visible, jnp.exp(scores - new_best[:, :, None]), 0.0)
        row_total = shrink * row_total + jnp.sum(weights, axis=2)
        row_accum = shrink[:, :, None] * row_accum + jnp.einsum(
            "hqk,khd->hqd",
            weights.astype(jnp.bfloat16),
            value_heads,
            preferred_element_type=jnp.float32,
        )
        return (new_best, row_total, row_accum)

    initial = tuple(
        (
            (
                jnp.full((heads_here, group[0].shape[0]), -1e30, jnp.float32),
                jnp.zeros((heads_here, group[0].shape[0]), jnp.float32),
                jnp.zeros((heads_here, group[0].shape[0], HEAD), jnp.float32),
            )
            for group in group_data
        )
    )
    key_group = lax.all_gather(key_rows, "sp", axis=0, tiled=True)
    value_group = lax.all_gather(value_rows, "sp", axis=0, tiled=True)
    length_in = key_group.shape[0]
    turns = length_in // local_rows

    def advance(turn_index, carry_now):
        begin_row = turn_index * local_rows
        key_block = lax.dynamic_slice_in_dim(key_group, begin_row, local_rows, 0)
        value_block = lax.dynamic_slice_in_dim(value_group, begin_row, local_rows, 0)
        updated = []
        for group, inner_carry in zip(group_data, carry_now):
            wanted = jnp.logical_and(begin_row <= group[3], begin_row + local_rows > 0)

            def take_block(inner, group=group):
                return absorb(inner, group, key_block, value_block, begin_row)

            def skip_block(inner):
                return inner

            updated.append(lax.cond(wanted, take_block, skip_block, inner_carry))
        return tuple(updated)

    carry = lax.fori_loop(0, turns, advance, initial)
    attended_parts = []
    total_parts = []
    for row_best, row_total, row_accum in carry:
        count_rows = row_total.shape[1]
        attended_parts.append(
            (row_accum / row_total[:, :, None])
            .astype(jnp.bfloat16)
            .transpose(1, 0, 2)
            .reshape(count_rows, width_att)
        )
        total_parts.append(row_best + jnp.log(row_total))
    attended = attended_parts[0]
    log_total = total_parts[0]
    rim_rows = shifted(gated[local_rows - (kernel_len - 1) :], "sp", 1)
    padded = jnp.concatenate([rim_rows, gated], axis=0).astype(jnp.float32)
    convolved = jnp.zeros((local_rows, channels), jnp.float32)
    for tap_index in range(kernel_len):
        convolved = (
            convolved + conv_taps[tap_index][None, :] * padded[tap_index : tap_index + local_rows]
        )
    all_channels = channels * lax.axis_size("tp")
    channel_square = lax.psum(jnp.sum(convolved * convolved, axis=1), "tp") / all_channels
    conv_out = jax.nn.silu(
        convolved * lax.rsqrt(channel_square + 1e-06)[:, None] * conv_gain[None, :]
    ).astype(jnp.bfloat16)
    group_part = jnp.dot(attended, out_attn, preferred_element_type=jnp.float32)
    group_part = group_part + jnp.dot(conv_out, out_conv, preferred_element_type=jnp.float32)
    mixed = lax.psum_scatter(
        lax.optimization_barrier(group_part.astype(jnp.bfloat16))
        .astype(jnp.float32)
        .astype(jnp.bfloat16),
        "tp",
        scatter_dimension=0,
        tiled=True,
    )
    return (mixed, log_total)


def solution(mesh):
    in_specs = (
        P(("sp", "tp"), None),
        P(),
        P(None, "tp"),
        P(None, "tp"),
        P(None, "tp"),
        P(None, "tp"),
        P(None, "tp"),
        P(None, "tp"),
        P("tp"),
        P("tp", None),
        P("tp", None),
        P("tp", None),
    )
    out_specs = (P(("sp", "tp"), None), P("tp", "sp"))
    return jax.shard_map(
        per_device, mesh=mesh, in_specs=in_specs, out_specs=out_specs, check_vma=False
    )
```

profile of v0, /device:TPU:0, one launch (start us, length us, event | category | flops | bytes accessed | tf_op | source)
XLA Modules:
  0.0 236.0 jit_solution(1296425185891095124)
XLA Ops:
  7.2 0.0 copy-start
  7.2 0.0 all-gather.4.cloned.1.call-start
  7.2 0.7 all-gather.4.cloned.1.call-update
  7.9 0.0 copy-start.5
  7.9 0.0 copy-start.7
  7.9 0.0 all-gather.6.cloned.1.call-start
  8.0 26.9 %all-gather.4.cloned.1.call-done = bf16[512,2048]{1,0:T(8,128)(2,1)} async-done(((bf16[128,2048]{1,0:T(8,128)(2,1)}), bf16[512,2048]{1,0:T(8,128)(2,1)}) %all-gather.4.cloned.1.call-update) | async-done | bytes 2097168 | tf_op jit(solution)/shard_map/all_gather | solution.py:33
  34.9 2.1 fusion.13
  37.0 3.3 %convolution_convert_fusion.1 = bf16[512,256]{1,0:T(8,128)(2,1)} fusion(bf16[2048,256]{1,0:T(8,128)(2,1)} %param.19, bf16[512,2048]{1,0:T(8,128)(2,1)} %all-gather.4.cloned.1.call-done, f32[2048]{0:T(1024)} %param.17, f32[512]{0:T(512)S(1)} %add_rsqrt_fusion.1), kind=kOutput, calls=%fused_computation.35 | convolution fusion | flops 541196288 | bytes 3418112 | tf_op jit(solution)/shard_map/dot_general | solution.py:39
  40.3 0.0 copy-start.3
  40.3 0.0 all-gather.6.cloned.1.call-update
  40.3 0.0 all-gather.8.cloned.1.call-start
  40.4 0.0 copy-done.5
  40.4 0.0 copy-done.7
  40.4 3.0 %convolution_convert_fusion = bf16[512,256]{1,0:T(8,128)(2,1)} fusion(bf16[2048,256]{1,0:T(8,128)(2,1)S(1)} %copy-done.5, bf16[512,2048]{1,0:T(8,128)(2,1)} %all-gather.4.cloned.1.call-done, f32[2048]{0:T(1024)S(1)} %copy-done.7, f32[512]{0:T(512)S(1)} %add_rsqrt_fusion.1), kind=kOutput, calls=%fused_computation.34 | convolution fusion | flops 541196288 | bytes 3418112 | tf_op jit(solution)/shard_map/dot_general | solution.py:40
  43.4 0.0 all-gather.8.cloned.1.call-update
  43.5 0.0 reduce-scatter.2.cloned.1.call-start
  43.5 0.7 constant_dynamic-slice_fusion.3
  44.2 0.0 copy-done.3
  44.3 0.0 copy-start.1
  44.3 0.0 copy-start.4
  44.3 3.8 %fusion.18 = f32[512,512]{1,0:T(8,128)S(1)} fusion(bf16[2048,512]{1,0:T(8,128)(2,1)} %param.22, bf16[512,2048]{1,0:T(8,128)(2,1)} %all-gather.4.cloned.1.call-done, f32[2048]{0:T(1024)S(1)} %copy-done.7, f32[512]{0:T(512)S(1)} %add_rsqrt_fusion.1), kind=kOutput, calls=%fused_computation.30 | convolution fusion | flops 1078722560 | bytes 5253120 | tf_op jit(solution)/shard_map/dot_general | solution.py:42
  48.1 0.0 copy-done.1
  48.1 0.0 copy-done.4
  48.1 0.0 copy-start.6
  48.2 1.3 fusion.19
  49.5 3.4 %collective-permute-start = (bf16[30,512]{1,0:T(8,128)(2,1)S(1)}, bf16[30,512]{1,0:T(8,128)(2,1)S(1)}, u32[]{:S(2)}, u32[]{:S(2)}) collective-permute-start(bf16[30,512]{1,0:T(8,128)(2,1)S(1)} %slice.252), channel_id=1, source_target_pairs={{0,4},{4,8},{8,12},{12,16},{16,20},{20,24},{24,28},{1,5},{5,9},{9,... | collective-permute-start | bytes 92168 | tf_op jit(solution)/shard_map/ppermute | solution.py:12
  52.9 0.0 copy-done.6
  52.9 1.0 fusion.20
  53.9 0.6 collective-permute-done
  54.5 0.2 maximum_convert_fusion
  54.6 5.7 %multiply_reduce_fusion = (f32[512]{0:T(512)S(1)}, f32[512,512]{1,0:T(8,128)}) fusion(f32[542,512]{1,0:T(8,128)S(1)} %maximum_convert_fusion, f32[512]{0:T(512)S(1)} %bitcast.72, f32[512]{0:T(512)S(1)} %bitcast.73, f32[512]{0:T(512)S(1)} %bitcast.75, f32[512]{0:T(512)S(1)} %bitcast.76, f32[512]{0:T(512)S(1)} %bitcast.77, f32[512]{0:T(512)S(1)} %bitcast.78, ...), kind=kLoop, calls=%fused_computation.98 | loop fusion | flops 16514560 | bytes 33619968 | tf_op jit(solution)/shard_map/reduce_sum | solution.py:147
  60.3 6.1 %psum.7 = f32[512]{0:T(512)S(1)} all-reduce(f32[512]{0:T(512)S(1)} %get-tuple-element.390), channel_id=1, replica_groups=mesh['sp'=8,'tp'=4] {'tp'}, use_global_device_ids=true, to_apply=%region_8.9 | all-reduce | flops 512 | bytes 4096 | tf_op jit(solution)/shard_map/psum | solution.py:147
  66.4 23.3 %all-gather.6.cloned.1.call-done = bf16[4096,256]{1,0:T(8,128)(2,1)} async-done(((bf16[512,256]{1,0:T(8,128)(2,1)}), bf16[4096,256]{1,0:T(8,128)(2,1)}) %all-gather.6.cloned.1.call-update) | async-done | bytes 2097168 | tf_op jit(solution)/shard_map/all_gather | solution.py:103
  89.7 4.1 %copy.15 = bf16[4096,256]{0,1:T(8,128)(2,1)} copy(bf16[4096,256]{1,0:T(8,128)(2,1)} %all-gather.6.cloned.1.call-done) | data formatting | bytes 4194304
  93.8 45.7 %all-gather.8.cloned.1.call-done = bf16[4096,256]{1,0:T(8,128)(2,1)} async-done(((bf16[512,256]{1,0:T(8,128)(2,1)}), bf16[4096,256]{1,0:T(8,128)(2,1)}) %all-gather.8.cloned.1.call-update) | async-done | bytes 2097168 | tf_op jit(solution)/shard_map/all_gather | solution.py:104
  139.5 4.1 %copy.16 = bf16[4096,256]{0,1:T(8,128)(2,1)} copy(bf16[4096,256]{1,0:T(8,128)(2,1)} %all-gather.8.cloned.1.call-done) | data formatting | bytes 4194304
  143.7 6.8 %while.18 = (s32[]{:T(128)}, f32[4,512]{1,0:T(4,128)S(1)}, f32[4,512]{1,0:T(4,128)S(1)}, f32[4,512,64]{1,2,0:T(8,128)S(1)}, s32[]{:T(128)}, /*index=5*/bf16[4096...) while((s32[]{:T(128)}, f32[4,512]{1,0:T(4,128)S(1)}, ...), condition=%wide.region_6.7_spmd.clone, body=%wide.region_1.6_spmd.clone.sunk | while | flops 286005248 | bytes 16725373 | solution.py:125
  143.8 6.3 %conditional.3 = ((f32[4,512]{1,0:T(4,128)S(1)}, f32[4,512]{1,0:T(4,128)S(1)}, f32[4,512,64]{1,2,0:T(8,128)S(1)})) conditional(s32[]{:T(128)} %convert_element_type.89, (f32[4,512]{1,0:T(4,128)S(1)}, f32[4,512]{1,0:T(4,128)S(1)}, f32[4,512,64]{1,2,0:T(8,128)S(1)}) %tuple.88, (s32[]{:T(128)}, s32[]{:T(128)}, bf16[4096,256]{0,1:T(8,128)(2,1)}, ...), branch_computations={%region_2.0_spmd, %region_3.5_spmd} | conditional | flops 286005248 | bytes 16723030 | solution.py:122
  143.8 0.2 compare_and_fusion
  144.1 0.7 constant_dynamic-slice_fusion.1
  144.8 1.1 constant_dynamic-slice_fusion
  145.8 1.2 fusion.4
  147.0 1.4 fusion.3
  148.4 1.6 fusion.8
  150.5 0.0 copy-start.2
  150.5 0.0 copy-start.8
  150.5 0.1 divide_convert_fusion
  150.6 2.0 fusion.63
  152.6 0.0 copy-done
  152.6 0.0 copy-done.2
  152.6 0.0 copy-done.8
  152.7 2.8 %add_convert_fusion = bf16[512,2048]{1,0:T(8,128)(2,1)} fusion(f32[512,2048]{1,0:T(8,128)S(1)} %fusion.63, bf16[512,2048]{1,0:T(8,128)(2,1)S(1)} %copy-done, f32[512,512]{1,0:T(8,128)S(1)} %copy-done.2, f32[512]{0:T(512)S(1)} %copy-done.8, f32[512]{0:T(512)S(1)} %add_rsqrt_fusion), kind=kOutput, calls=%fused_computation.25 | convolution fusion | flops 1077673984 | bytes 9441280 | tf_op jit(solution)/shard_map/dot_general | solution.py:152
  155.5 0.0 reduce-scatter.2.cloned.1.call-update
  155.5 0.6 log_add_fusion
  156.1 73.3 %reduce-scatter.2.cloned.1.call-done = bf16[128,2048]{1,0:T(8,128)(2,1)} async-done(((bf16[512,2048]{1,0:T(8,128)(2,1)}), bf16[128,2048]{1,0:T(8,128)(2,1)}) %reduce-scatter.2.cloned.1.call-update) | async-done | bytes 524304 | tf_op jit(solution)/shard_map/reduce_scatter | solution.py:153
  (28 shorter events, 0.3 us)
Async XLA Ops:
  7.2 145.5 %copy-start = (bf16[512,2048]{1,0:T(8,128)(2,1)S(1)}, bf16[512,2048]{1,0:T(8,128)(2,1)}, u32[]{:S(2)}) copy-start(bf16[512,2048]{1,0:T(8,128)(2,1)} %param.27) | copy-start | bytes 6291460
  7.2 27.7 %all-gather.4.cloned.1.call-start = ((), (), s32[]{:S(2)}) async-start(), calls=%async_computation.1 | async-start | bytes 2621440 | tf_op jit(solution)/shard_map/all_gather | solution.py:33
  7.9 32.5 %copy-start.5 = (bf16[2048,256]{1,0:T(8,128)(2,1)S(1)}, bf16[2048,256]{1,0:T(8,128)(2,1)}, u32[]{:S(2)}) copy-start(bf16[2048,256]{1,0:T(8,128)(2,1)} %param.20) | copy-start | bytes 3145732
  7.9 32.5 %copy-start.7 = (f32[2048]{0:T(1024)S(1)}, f32[2048]{0:T(1024)}, u32[]{:S(2)}) copy-start(f32[2048]{0:T(1024)} %param.17) | copy-start | bytes 24580
  7.9 81.8 %all-gather.6.cloned.1.call-start = ((), (), s32[]{:S(2)}) async-start(), calls=%async_computation.2 | async-start | bytes 2359296 | tf_op jit(solution)/shard_map/all_gather | solution.py:103
  40.3 3.9 %copy-start.3 = (f32[31,512]{1,0:T(8,128)S(1)}, f32[31,512]{1,0:T(8,128)}, u32[]{:S(2)}) copy-start(f32[31,512]{1,0:T(8,128)} %param.23) | copy-start | bytes 190468
  40.3 99.2 %all-gather.8.cloned.1.call-start = ((), (), s32[]{:S(2)}) async-start(), calls=%async_computation.3 | async-start | bytes 2359296 | tf_op jit(solution)/shard_map/all_gather | solution.py:104
  43.5 186.0 %reduce-scatter.2.cloned.1.call-start = ((), (), s32[]{:S(2)}) async-start(), calls=%async_computation.4 | async-start | bytes 2621440 | tf_op jit(solution)/shard_map/reduce_scatter | solution.py:153
  44.3 3.8 %copy-start.1 = (bf16[512,2048]{1,0:T(8,128)(2,1)S(1)}, bf16[512,2048]{1,0:T(8,128)(2,1)}, u32[]{:S(2)}) copy-start(bf16[512,2048]{1,0:T(8,128)(2,1)} %all-gather.4.cloned.1.call-done) | copy-start | bytes 6291460
  44.3 3.8 %copy-start.4 = (bf16[2048,512]{1,0:T(8,128)(2,1)S(1)}, bf16[2048,512]{1,0:T(8,128)(2,1)}, u32[]{:S(2)}) copy-start(bf16[2048,512]{1,0:T(8,128)(2,1)} %param.21) | copy-start | bytes 6291460
  48.1 4.7 %copy-start.6 = (bf16[2048,256]{1,0:T(8,128)(2,1)S(1)}, bf16[2048,256]{1,0:T(8,128)(2,1)}, u32[]{:S(2)}) copy-start(bf16[2048,256]{1,0:T(8,128)(2,1)} %param.18) | copy-start | bytes 3145732
  49.5 5.0 %collective-permute-start = (bf16[30,512]{1,0:T(8,128)(2,1)S(1)}, bf16[30,512]{1,0:T(8,128)(2,1)S(1)}, u32[]{:S(2)}, u32[]{:S(2)}) collective-permute-start(bf16[30,512]{1,0:T(8,128)(2,1)S(1)} %slice.252), channel_id=1, source_target_pairs={{0,4},{4,8},{8,12},{12,16},{16,20},{20,24},{24,28},{1,5},{5,9},{9,... | collective-permute-start | bytes 92168 | tf_op jit(solution)/shard_map/ppermute | solution.py:12
  150.5 2.1 copy-start.2
  150.5 2.1 copy-start.8
Sparse Core Ops, SparseCore 0:
  9.5 25.2 all-gather.3
  40.4 49.2 all-gather.5
  91.9 47.6 all-gather.7
  155.6 73.7 reduce-scatter.1
where the time goes:
time: 237 us; the launch traced here: 236 us
  waiting for transfers between devices  171 us (72%)
  matrix products  20.1 us (8%)
  between operations  14 us (6%)
  local copies, waits for them, and re-layouts  10.9 us (5%)
  other arithmetic  10.3 us (4%)
  blocking collectives  6.08 us (3%)
  starting transfers between devices  3.54 us (1%)
    reduce_scatter x1, waiting for transfers between devices, per_device(): lax.psum_scatter(lax.optimization_barrier(group_part.astype(jnp.bfloat16)...  73.3 us
    all_gather x1, waiting for transfers between devices, per_device(): value_group = lax.all_gather(value_rows, 'sp', axis=0, tiled=True)  45.7 us
    all_gather x1, waiting for transfers between devices, per_device(): wide = lax.all_gather(tokens, 'tp', axis=0, tiled=True).astype(jnp.float32)  26.9 us
    all_gather x1, waiting for transfers between devices, per_device(): key_group = lax.all_gather(key_rows, 'sp', axis=0, tiled=True)  23.3 us
    unnamed x20, local copies, waits for them, and re-layouts  8.28 us
    psum x1, blocking collectives, per_device(): lax.psum(jnp.sum(convolved * convolved, axis=1), 'tp') / all_channels  6.08 us
    reduce_sum x1, other arithmetic, per_device(): jnp.sum(convolved * convolved, axis=1)  5.69 us
  transfers between devices with their start and end apart: 5, of which 5 were waited for; matrix products, arithmetic and copies ran while one was open for 9% of the time, Pallas kernels for 0%

commit v1 on v0

--- a/solution.py
+++ b/solution.py
@@ -1,9 +1,23 @@
+import functools
 import jax
 import jax.numpy as jnp
 from jax import lax
 from jax.sharding import PartitionSpec as P
 
 HEAD = 64
+
+
+def goods_perform(x0, where_dim):
+    pages = []
+    for _ in range(jax.lax.axis_size("tp")):
+        pages.append(x0)
+    return jnp.concatenate(
+        jax.lax.all_to_all(jnp.stack(pages), axis_name="tp", split_axis=0, concat_axis=0),
+        axis=where_dim,
+    )
+
+
+perform_zones = functools.partial(goods_perform, where_dim=0)
 
 
 def shifted(array, axis, by):
@@ -30,7 +44,7 @@
     width_att = w_query.shape[1]
     channels = conv_in.shape[1]
     kernel_len = conv_taps.shape[0]
-    wide = lax.all_gather(tokens, "tp", axis=0, tiled=True).astype(jnp.float32)
+    wide = perform_zones(tokens).astype(jnp.float32)
     factor = lax.rsqrt(jnp.mean(wide * wide, axis=1, keepdims=True) + 1e-06)
     normed = (wide * factor * norm_gain[None, :]).astype(jnp.bfloat16)
     query = (jnp.dot(normed, w_query, preferred_element_type=jnp.float32) * HEAD ** (-0.5)).astype(

time: 237 us -> 239 us (level)
  blocking collectives: 6.08 us -> 35.7 us
  waiting for transfers between devices: 171 us -> 144 us
  local copies, waits for them, and re-layouts: 10.9 us -> 13.9 us
    all_to_all x0 -> x1, blocking collectives: none -> 29.7 us  [goods_perform(): jax.lax.all_to_all(jnp.stack(pages), axis_name='tp', split_axis=0, concat...]
    all_gather x1 -> x0, waiting for transfers between devices: 26.9 us -> none  [per_device(): wide = lax.all_gather(tokens, 'tp', axis=0, tiled=True).astype(jnp.float32)]
    unnamed x20 -> x24, local copies, waits for them, and re-layouts: 8.28 us -> 9.83 us
  transfers between devices with their start and end apart: 5 -> 4, of which waited for: 5 -> 4; matrix products, arithmetic and copies ran while one was open for 9% -> 8% of each run, Pallas kernels for 0% -> 0%
where the time goes in v1:
time: 239 us; the launch traced here: 238 us
  waiting for transfers between devices  144 us (60%)
  blocking collectives  35.7 us (15%)
  matrix products  17.9 us (7%)
  between operations  14 us (6%)
  local copies, waits for them, and re-layouts  13.9 us (6%)
  other arithmetic  9.23 us (4%)
  starting transfers between devices  3.52 us (1%)
    reduce_scatter x1, waiting for transfers between devices, per_device(): lax.psum_scatter(lax.optimization_barrier(group_part.astype(jnp.bfloat16)...  73.3 us
    all_gather x1, waiting for transfers between devices, per_device(): value_group = lax.all_gather(value_rows, 'sp', axis=0, tiled=True)  45.7 us
    all_to_all x1, blocking collectives, goods_perform(): jax.lax.all_to_all(jnp.stack(pages), axis_name='tp', split_axis=0, concat...  29.7 us
    all_gather x1, waiting for transfers between devices, per_device(): key_group = lax.all_gather(key_rows, 'sp', axis=0, tiled=True)  23.9 us
    unnamed x24, local copies, waits for them, and re-layouts  9.83 us
    psum x1, blocking collectives, per_device(): lax.psum(jnp.sum(convolved * convolved, axis=1), 'tp') / all_channels  5.92 us
    reduce_sum x1, other arithmetic, per_device(): jnp.sum(convolved * convolved, axis=1)  5.69 us
  transfers between devices with their start and end apart: 4, of which 4 were waited for; matrix products, arithmetic and copies ran while one was open for 8% of the time, Pallas kernels for 0%

profile of v1, /device:TPU:0, one launch (start us, length us, event | category | flops | bytes accessed | tf_op | source)
XLA Modules:
  0.0 238.4 jit_solution(16830933884112938600)
XLA Ops:
  7.2 0.0 copy-start
  7.2 0.0 all-gather.3.cloned.1.call-start
  7.2 1.4 stack.2
  8.7 29.7 %all_to_all.5 = bf16[4,128,2048]{2,1,0:T(8,128)(2,1)S(1)} all-to-all(bf16[4,128,2048]{2,1,0:T(8,128)(2,1)S(1)} %stack.2), channel_id=1, replica_groups=mesh['sp'=8,'tp'=4] {'tp'}, dimensions={0} | all-to-all | bytes 4194304 | tf_op jit(solution)/shard_map/all_to_all | solution.py:15
  38.4 0.0 copy-start.5
  38.4 0.5 multiply_reduce_fusion
  38.9 0.2 copy-done.5
  39.1 0.0 copy-start.7
  39.1 0.5 fusion.14
  39.6 0.0 copy-start.1
  39.6 1.3 copy-done.1
  41.0 0.0 copy-done.7
  41.0 0.0 copy-start.8
  41.0 1.4 convolution_convert_fusion.1
  42.4 0.0 all-gather.3.cloned.1.call-update
  42.4 0.0 copy-start.4
  42.4 0.0 all-gather.5.cloned.1.call-start
  42.5 0.0 copy-done.8
  42.5 3.0 %convolution_convert_fusion = bf16[512,256]{1,0:T(8,128)(2,1)} fusion(bf16[512,2048]{1,0:T(8,128)(2,1)} %copy-done.1, bf16[2048,256]{1,0:T(8,128)(2,1)S(1)} %copy-done.8), kind=kOutput, calls=%fused_computation.33 | convolution fusion | flops 537001984 | bytes 3407872 | tf_op jit(solution)/shard_map/dot_general | solution.py:54
  45.5 0.0 all-gather.5.cloned.1.call-update
  45.5 0.0 reduce-scatter.2.cloned.1.call-start
  45.6 0.7 constant_dynamic-slice_fusion.3
  46.3 0.0 copy-done.4
  46.3 0.0 copy-start.2
  46.3 0.0 copy-start.6
  46.4 3.8 %fusion.17 = f32[512,512]{1,0:T(8,128)S(1)} fusion(bf16[512,2048]{1,0:T(8,128)(2,1)} %copy-done.1, bf16[2048,512]{1,0:T(8,128)(2,1)} %param.22), kind=kOutput, calls=%fused_computation.29 | convolution fusion | flops 1074528256 | bytes 5242880 | tf_op jit(solution)/shard_map/dot_general | solution.py:56
  50.1 0.0 copy-done.2
  50.1 0.0 copy-done.6
  50.1 0.0 copy-start.9
  50.2 1.3 fusion.18
  51.4 3.4 %collective-permute-start = (bf16[30,512]{1,0:T(8,128)(2,1)S(1)}, bf16[30,512]{1,0:T(8,128)(2,1)S(1)}, u32[]{:S(2)}, u32[]{:S(2)}) collective-permute-start(bf16[30,512]{1,0:T(8,128)(2,1)S(1)} %slice.252), channel_id=1, source_target_pairs={{0,4},{4,8},{8,12},{12,16},{16,20},{20,24},{24,28},{1,5},{5,9},{9,... | collective-permute-start | bytes 92168 | tf_op jit(solution)/shard_map/ppermute | solution.py:26
  54.8 0.0 copy-done.9
  54.9 0.8 fusion.19
  55.6 0.8 collective-permute-done
  56.4 0.2 maximum_convert_fusion
  56.6 5.7 %multiply_reduce_fusion.1 = (f32[512]{0:T(512)S(1)}, f32[512,512]{1,0:T(8,128)}) fusion(f32[542,512]{1,0:T(8,128)S(1)} %maximum_convert_fusion, f32[512]{0:T(512)S(1)} %bitcast.85, f32[512]{0:T(512)S(1)} %bitcast.86, f32[512]{0:T(512)S(1)} %bitcast.88, f32[512]{0:T(512)S(1)} %bitcast.89, f32[512]{0:T(512)S(1)} %bitcast.90, f32[512]{0:T(512)S(1)} %bitcast.91, ...), kind=kLoop, calls=%fused_computation.97 | loop fusion | flops 16514560 | bytes 33619968 | tf_op jit(solution)/shard_map/reduce_sum | solution.py:161
  62.3 5.9 %psum.7 = f32[512]{0:T(512)S(1)} all-reduce(f32[512]{0:T(512)S(1)} %get-tuple-element.401), channel_id=1, replica_groups=mesh['sp'=8,'tp'=4] {'tp'}, use_global_device_ids=true, to_apply=%region_8.9 | all-reduce | flops 512 | bytes 4096 | tf_op jit(solution)/shard_map/psum | solution.py:161
  68.2 23.9 %all-gather.3.cloned.1.call-done = bf16[4096,256]{1,0:T(8,128)(2,1)} async-done(((bf16[512,256]{1,0:T(8,128)(2,1)}), bf16[4096,256]{1,0:T(8,128)(2,1)}) %all-gather.3.cloned.1.call-update) | async-done | bytes 2097168 | tf_op jit(solution)/shard_map/all_gather | solution.py:117
  92.1 4.1 %copy.18 = bf16[4096,256]{0,1:T(8,128)(2,1)} copy(bf16[4096,256]{1,0:T(8,128)(2,1)} %all-gather.3.cloned.1.call-done) | data formatting | bytes 4194304
  96.2 45.7 %all-gather.5.cloned.1.call-done = bf16[4096,256]{1,0:T(8,128)(2,1)} async-done(((bf16[512,256]{1,0:T(8,128)(2,1)}), bf16[4096,256]{1,0:T(8,128)(2,1)}) %all-gather.5.cloned.1.call-update) | async-done | bytes 2097168 | tf_op jit(solution)/shard_map/all_gather | solution.py:118
  141.9 4.1 %copy.19 = bf16[4096,256]{0,1:T(8,128)(2,1)} copy(bf16[4096,256]{1,0:T(8,128)(2,1)} %all-gather.5.cloned.1.call-done) | data formatting | bytes 4194304
  146.1 6.8 %while.18 = (s32[]{:T(128)}, f32[4,512]{1,0:T(4,128)S(1)}, f32[4,512]{1,0:T(4,128)S(1)}, f32[4,512,64]{1,2,0:T(8,128)S(1)}, s32[]{:T(128)}, /*index=5*/bf16[4096...) while((s32[]{:T(128)}, f32[4,512]{1,0:T(4,128)S(1)}, ...), condition=%wide.region_6.7_spmd.clone, body=%wide.region_1.6_spmd.clone.sunk | while | flops 286005248 | bytes 16725373 | solution.py:139
  146.2 6.3 %conditional.3 = ((f32[4,512]{1,0:T(4,128)S(1)}, f32[4,512]{1,0:T(4,128)S(1)}, f32[4,512,64]{1,2,0:T(8,128)S(1)})) conditional(s32[]{:T(128)} %convert_element_type.82, (f32[4,512]{1,0:T(4,128)S(1)}, f32[4,512]{1,0:T(4,128)S(1)}, f32[4,512,64]{1,2,0:T(8,128)S(1)}) %tuple.89, (s32[]{:T(128)}, s32[]{:T(128)}, bf16[4096,256]{0,1:T(8,128)(2,1)}, ...), branch_computations={%region_2.0_spmd, %region_3.5_spmd} | conditional | flops 286005248 | bytes 16723030 | solution.py:136
  146.2 0.2 compare_and_fusion
  146.5 0.7 constant_dynamic-slice_fusion.1
  147.2 1.1 constant_dynamic-slice_fusion
  148.2 1.2 fusion.4
  149.4 1.4 fusion.3
  150.8 1.6 fusion.8
  152.9 0.1 divide_convert_fusion
  153.0 0.0 copy-start.3
  153.0 0.0 copy-start.10
  153.0 2.0 fusion.57
  155.0 0.0 copy-done
  155.0 0.0 copy-done.3
  155.1 0.0 copy-done.10
  155.1 2.8 %add_convert_fusion = bf16[512,2048]{1,0:T(8,128)(2,1)} fusion(f32[512,2048]{1,0:T(8,128)S(1)} %fusion.57, bf16[512,2048]{1,0:T(8,128)(2,1)S(1)} %copy-done, f32[512,512]{1,0:T(8,128)S(1)} %copy-done.3, f32[512]{0:T(512)S(1)} %copy-done.10, f32[512]{0:T(512)S(1)} %add_rsqrt_fusion), kind=kOutput, calls=%fused_computation.23 | convolution fusion | flops 1077673984 | bytes 9441280 | tf_op jit(solution)/shard_map/dot_general | solution.py:166
  157.9 0.0 reduce-scatter.2.cloned.1.call-update
  157.9 0.6 log_add_fusion
  158.5 73.3 %reduce-scatter.2.cloned.1.call-done = bf16[128,2048]{1,0:T(8,128)(2,1)} async-done(((bf16[512,2048]{1,0:T(8,128)(2,1)}), bf16[128,2048]{1,0:T(8,128)(2,1)}) %reduce-scatter.2.cloned.1.call-update) | async-done | bytes 524304 | tf_op jit(solution)/shard_map/reduce_scatter | solution.py:167
  (28 shorter events, 0.3 us)
Async XLA Ops:
  7.2 147.9 %copy-start = (bf16[512,2048]{1,0:T(8,128)(2,1)S(1)}, bf16[512,2048]{1,0:T(8,128)(2,1)}, u32[]{:S(2)}) copy-start(bf16[512,2048]{1,0:T(8,128)(2,1)} %param.27) | copy-start | bytes 6291460
  7.2 84.9 %all-gather.3.cloned.1.call-start = ((), (), s32[]{:S(2)}) async-start(), calls=%async_computation.2 | async-start | bytes 2359296 | tf_op jit(solution)/shard_map/all_gather | solution.py:117
  38.4 0.7 copy-start.5
  39.1 1.9 copy-start.7
  39.6 1.3 copy-start.1
  41.0 1.5 copy-start.8
  42.4 3.9 %copy-start.4 = (f32[31,512]{1,0:T(8,128)S(1)}, f32[31,512]{1,0:T(8,128)}, u32[]{:S(2)}) copy-start(f32[31,512]{1,0:T(8,128)} %param.23) | copy-start | bytes 190468
  42.4 99.5 %all-gather.5.cloned.1.call-start = ((), (), s32[]{:S(2)}) async-start(), calls=%async_computation.3 | async-start | bytes 2359296 | tf_op jit(solution)/shard_map/all_gather | solution.py:118
  45.5 186.4 %reduce-scatter.2.cloned.1.call-start = ((), (), s32[]{:S(2)}) async-start(), calls=%async_computation.4 | async-start | bytes 2621440 | tf_op jit(solution)/shard_map/reduce_scatter | solution.py:167
  46.3 3.8 %copy-start.2 = (bf16[512,2048]{1,0:T(8,128)(2,1)S(1)}, bf16[512,2048]{1,0:T(8,128)(2,1)}, u32[]{:S(2)}) copy-start(bf16[512,2048]{1,0:T(8,128)(2,1)} %copy-done.1) | copy-start | bytes 6291460
  46.3 3.8 %copy-start.6 = (bf16[2048,512]{1,0:T(8,128)(2,1)S(1)}, bf16[2048,512]{1,0:T(8,128)(2,1)}, u32[]{:S(2)}) copy-start(bf16[2048,512]{1,0:T(8,128)(2,1)} %param.21) | copy-start | bytes 6291460
  50.1 4.7 %copy-start.9 = (bf16[2048,256]{1,0:T(8,128)(2,1)S(1)}, bf16[2048,256]{1,0:T(8,128)(2,1)}, u32[]{:S(2)}) copy-start(bf16[2048,256]{1,0:T(8,128)(2,1)} %param.18) | copy-start | bytes 3145732
  51.4 5.0 %collective-permute-start = (bf16[30,512]{1,0:T(8,128)(2,1)S(1)}, bf16[30,512]{1,0:T(8,128)(2,1)S(1)}, u32[]{:S(2)}, u32[]{:S(2)}) collective-permute-start(bf16[30,512]{1,0:T(8,128)(2,1)S(1)} %slice.252), channel_id=1, source_target_pairs={{0,4},{4,8},{8,12},{12,16},{16,20},{20,24},{24,28},{1,5},{5,9},{9,... | collective-permute-start | bytes 92168 | tf_op jit(solution)/shard_map/ppermute | solution.py:26
  153.0 2.1 copy-start.3
  153.0 2.1 copy-start.10
Sparse Core Ops, SparseCore 0:
  42.5 49.5 all-gather.2
  94.3 47.6 all-gather.4
  158.1 73.7 reduce-scatter.1
